TPU v7x, 256 devices: a 4x2x16 block of a 4x16x16 slice. The times are simulated.
256 devices in a mesh: grp: 2 (over y), ep: 64 (over z, x), tp: 2 (over core).
Axes of the slice: x: 4, y: 2, z: 16, core: 2. Of those that a mesh axis runs over, the one named last changes fastest.
The devices are a block of a 4x16x16 slice.
Arguments:
- hidden_state: bfloat16 [8192, 1024], P(('grp', 'ep'), 'tp'), parts along dimension 0, may hold values from -6 to 6
- expert_ids: int32 [8192, 4], P(('grp', 'ep')), parts along dimension 0, may hold values from 0 to 63, all different within a row; in each aligned block of 64 rows (0 to 63, 64 to 127, ...) at most 8 rows name the same one
- route_weight: float32 [8192, 4], P(('grp', 'ep')), parts along dimension 0, may hold values from 0.1 to 1
- gate_matrix: bfloat16 [64, 1024, 2048], P('ep', None, 'tp'), may hold values from -0.1875 to 0.1875
- up_matrix: bfloat16 [64, 1024, 2048], P('ep', None, 'tp'), may hold values from -0.1875 to 0.1875
- down_matrix: bfloat16 [64, 2048, 1024], P('ep', 'tp'), may hold values from -2 to 2
- norm_gain: float32 [1024], P('tp'), may hold values from 0.1 to 1.9
Outputs:
- normed_out: bfloat16 [8192, 1024], P(('grp', 'ep'), 'tp'), parts along dimension 0
There are 2 independent parts, one for each index of `grp`. A program takes and returns all parts, laid end to end along the dimension named above; an argument that names none is the same for every part. Nothing has to cross between parts.
Inputs may be any that keep to these rules, and one draw needn't show every extreme that they name: `expert_ids`: each row names 4 different experts. Within the rows of one index of ep (aligned blocks of 64 rows) no expert is named by more than 8 rows, and in some blocks one expert is named by exactly 8 rows. Every expert is named by some row.
All inputs are finite; a program needn't handle non-finite values.
Results may differ from a plain program's by a relative error of at most 0.0065.
Values may be sent and summed in bfloat16 or wider, within the bound.
A program may use at most 64 MiB of HBM per device.

v0:
```python
import jax
import jax.numpy as jnp
from jax import lax
from jax.sharding import PartitionSpec as P

D = 1024


norm_eps = 1e-05


def in_blocks(array, dim, length):
    before, after = (array.shape[:dim], array.shape[dim + 1 :])
    return jnp.moveaxis(array.reshape(*before, length, -1, *after), dim, 0)


def sum_at_owner(array, axis, dim):
    length = lax.axis_size(axis)
    parts = lax.all_to_all(in_blocks(array, dim, length), axis, 0, 0, tiled=True)
    return jnp.sum(parts.astype(jnp.float32), axis=0)


def laid_out(parts, dim):
    shape = list(parts.shape[1:])
    shape[dim] *= parts.shape[0]
    return jnp.moveaxis(parts, 0, dim).reshape(shape)


def copy_for_each(array, axis):
    length = lax.axis_size(axis)
    return lax.all_to_all(
        jnp.broadcast_to(array[None], (length, *array.shape)), axis, 0, 0, tiled=True
    )


def collect(array, axis, dim):
    return laid_out(copy_for_each(array, axis), dim)


def slot_numbers(block_ids, expert_count):
    onehot = (block_ids[..., None] == jnp.arange(expert_count, dtype=jnp.int32)).astype(jnp.int32)
    earlier = jnp.cumsum(onehot, axis=-2) - onehot
    return jnp.sum(earlier * onehot, axis=-1)


def expert_rows(buffer, gate_matrix, up_matrix, down_matrix):
    sources, item_count, feature_count = buffer.shape
    token_rows = buffer.reshape(sources * item_count, feature_count)
    gate_pre = jnp.dot(token_rows, gate_matrix[0], preferred_element_type=jnp.float32)
    up_pre = jnp.dot(token_rows, up_matrix[0], preferred_element_type=jnp.float32)
    activated = (jax.nn.silu(gate_pre) * up_pre).astype(jnp.bfloat16)
    partial_value = jnp.dot(activated, down_matrix[0], preferred_element_type=jnp.float32)
    summed = sum_at_owner(
        partial_value.reshape(sources, item_count, feature_count).astype(jnp.bfloat16), "tp", 2
    )
    return summed.astype(jnp.bfloat16)


def shards(hidden_state, expert_ids, route_weight, gate_matrix, up_matrix, down_matrix, norm_gain):
    tok_count, top_count = expert_ids.shape
    expert_count = lax.axis_size("ep")
    capacity = max(2, 2 * tok_count * top_count // expert_count)
    slot_total = expert_count * capacity
    slot_rank = slot_numbers(expert_ids.reshape(1, tok_count * top_count), expert_count)
    slot_index = expert_ids * capacity + slot_rank.reshape(tok_count, top_count)
    positions = jnp.arange(slot_total, dtype=jnp.int32)
    matches = slot_index[:, :, None] == positions[None, None, :]
    placing = jnp.transpose(jnp.any(matches, axis=1)).astype(jnp.bfloat16)
    combine = jnp.sum(jnp.where(matches, route_weight[:, :, None], 0.0), axis=1)
    outgoing = jnp.dot(placing, hidden_state, preferred_element_type=jnp.float32).astype(
        jnp.bfloat16
    )
    answers = expert_rows(
        collect(
            lax.all_to_all(
                outgoing.reshape(expert_count, capacity, hidden_state.shape[1]),
                "ep",
                split_axis=0,
                concat_axis=0,
                tiled=True,
            ),
            "tp",
            2,
        ),
        gate_matrix,
        up_matrix,
        down_matrix,
    )
    returned = lax.all_to_all(answers, "ep", split_axis=0, concat_axis=0, tiled=True)
    combined = jnp.dot(
        combine,
        returned.reshape(slot_total, returned.shape[2]).astype(jnp.float32),
        precision=lax.Precision.HIGHEST,
    )
    local_squares = jnp.sum(combined * combined, axis=1)
    total_squares = lax.psum(local_squares, "tp")
    inverse_rms = lax.rsqrt(total_squares / D + norm_eps)
    return (combined * inverse_rms[:, None] * norm_gain).astype(jnp.bfloat16)


def solution(mesh):
    placed = (
        P(("grp", "ep"), "tp"),
        P(("grp", "ep"), None),
        P(("grp", "ep"), None),
        P("ep", None, "tp"),
        P("ep", None, "tp"),
        P("ep", "tp", None),
        P("tp"),
    )
    return jax.shard_map(
        shards, mesh=mesh, in_specs=placed, out_specs=P(("grp", "ep"), "tp"), check_vma=False
    )
```

profile of v0, /device:TPU:33, one launch (start us, length us, event | category | flops | bytes accessed | tf_op | source)
XLA Modules:
  0.0 130.7 jit_solution(2665535708443496300)
XLA Ops:
  0.0 0.9 copy.35
  1.1 0.6 reduce-window.6
  1.7 0.2 slice_reduce_fusion
  2.1 0.1 broadcast.56
  2.2 0.1 fusion.20
  2.4 0.1 reshape.140
  2.6 0.7 multiply_add_fusion
  3.3 0.1 fusion.19
  3.4 1.2 fusion.14
  4.6 58.4 %all_to_all.20 = bf16[64,8,512]{2,1,0:T(8,128)(2,1)S(1)} all-to-all(bf16[64,8,512]{2,1,0:T(8,128)(2,1)S(1)} %fusion.14), channel_id=1, replica_groups=mesh['grp'=2,'ep'=64,'tp'=2] {'ep'}, dimensions={0} | all-to-all | bytes 1048576 | tf_op jit(solution)/shard_map/all_to_all | solution.py:75
  63.0 7.5 %all_to_all.21 = bf16[2,64,8,512]{3,2,1,0:T(8,128)(2,1)S(1)} all-to-all(bf16[2,64,8,512]{3,2,1,0:T(8,128)(2,1)S(1)} %broadcast_in_dim.16), channel_id=1, replica_groups=mesh['grp'=2,'ep'=64,'tp'=2] {'tp'}, dimensions={0} | all-to-all | bytes 2097152 | tf_op jit(solution)/shard_map/all_to_all | solution.py:31
  70.6 1.1 copy.46
  71.7 0.2 copy.42
  71.9 2.6 %fusion.4 = f32[512,1024]{1,0:T(8,128)} fusion(bf16[512,1024]{1,0:T(8,128)(2,1)S(1)} %bitcast.60, bf16[1,1024,1024]{2,1,0:T(8,128)(2,1)S(1)} %copy-done), kind=kOutput, calls=%fused_computation.4 | convolution fusion | flops 1073741824 | bytes 5242880 | tf_op jit(solution)/shard_map/dot_general | solution.py:49
  74.5 6.2 %fusion.8 = bf16[64,8,1024]{2,1,0:T(8,128)(2,1)} fusion(bf16[1,1024,1024]{2,1,0:T(8,128)(2,1)} %param.12, bf16[512,1024]{1,0:T(8,128)(2,1)S(1)} %bitcast.61, bf16[1,1024,1024]{2,1,0:T(8,128)(2,1)} %param.11, f32[512,1024]{1,0:T(8,128)} %fusion.4), kind=kOutput, calls=%fused_computation.7 | convolution fusion | flops 2151153664 | bytes 8388608 | tf_op jit(solution)/shard_map/dot_general | solution.py:52
  80.8 1.3 copy.45
  82.1 4.6 %all_to_all.22 = bf16[2,64,8,512]{3,2,1,0:T(8,128)(2,1)S(1)} all-to-all(bf16[2,64,8,512]{3,2,1,0:T(8,128)(2,1)S(1)} %bitcast.59), channel_id=1, replica_groups=mesh['grp'=2,'ep'=64,'tp'=2] {'tp'}, dimensions={0} | all-to-all | bytes 2097152 | tf_op jit(solution)/shard_map/all_to_all | solution.py:19
  86.7 1.1 reduce_sum.41
  87.8 7.2 %all-to-all-start.3 = ((bf16[64,8,512]{2,1,0:T(8,128)(2,1)}), bf16[64,8,512]{2,1,0:T(8,128)(2,1)S(1)}, u32[]{:S(2)}, u32[]{:S(2)}) async-start(bf16[64,8,512]{2,1,0:T(8,128)(2,1)} %reduce_sum.41), calls=%async_computation.3 | async-start | bytes 1048576 | tf_op jit(solution)/shard_map/all_to_all | solution.py:89
  95.0 0.1 select_reduce_fusion
  95.1 29.4 %all-to-all-done.3 = bf16[64,8,512]{2,1,0:T(8,128)(2,1)S(1)} async-done(((bf16[64,8,512]{2,1,0:T(8,128)(2,1)}), bf16[64,8,512]{2,1,0:T(8,128)(2,1)S(1)}, u32[]{:S(2)}, u32[]{:S(2)}) %all-to-all-start.3) | async-done | bytes 524320 | tf_op jit(solution)/shard_map/all_to_all | solution.py:89
  124.5 0.5 multiply_reduce_fusion
  125.0 5.0 %psum.7 = f32[64]{0:T(128)S(1)} all-reduce(f32[64]{0:T(128)S(1)} %get-tuple-element.5), channel_id=1, replica_groups=mesh['grp'=2,'ep'=64,'tp'=2] {'tp'}, use_global_device_ids=true, to_apply=%region_7.8 | all-reduce | flops 64 | bytes 512 | tf_op jit(solution)/shard_map/psum | solution.py:96
  129.9 0.7 multiply_convert_fusion.1
  (16 shorter events, 0.5 us)
Async XLA Ops:
  0.0 71.9 %copy-start = (bf16[1,1024,1024]{2,1,0:T(8,128)(2,1)S(1)}, bf16[1,1024,1024]{2,1,0:T(8,128)(2,1)}, u32[]{:S(2)}) copy-start(bf16[1,1024,1024]{2,1,0:T(8,128)(2,1)} %param.10) | copy-start | bytes 6291460
  82.1 12.9 %copy-start.1 = (f32[64,4]{0,1:T(4,128)S(1)}, f32[64,4]{0,1:T(4,128)}, u32[]{:S(2)}) copy-start(f32[64,4]{0,1:T(4,128)} %param.9) | copy-start | bytes 3076
  86.7 43.3 %copy-start.2 = (f32[512]{0:T(512)S(1)}, f32[512]{0:T(512)}, u32[]{:S(2)}) copy-start(f32[512]{0:T(512)} %param.13) | copy-start | bytes 6148
  87.8 36.7 %all-to-all-start.3 = ((bf16[64,8,512]{2,1,0:T(8,128)(2,1)}), bf16[64,8,512]{2,1,0:T(8,128)(2,1)S(1)}, u32[]{:S(2)}, u32[]{:S(2)}) async-start(bf16[64,8,512]{2,1,0:T(8,128)(2,1)} %reduce_sum.41), calls=%async_computation.3 | async-start | bytes 1048576 | tf_op jit(solution)/shard_map/all_to_all | solution.py:89
where the time goes:
time: 131 us
  blocking collectives  75.4 us (58%)
  waiting for transfers between devices  29.4 us (22%)
  matrix products  10.5 us (8%)
  starting transfers between devices  7.18 us (5%)
  local copies, waits for them, and re-layouts  4.38 us (3%)
  other arithmetic  3.66 us (3%)
    all_to_all x1, blocking collectives, shards(): lax.all_to_all(outgoing.reshape(expert_count, capacity, hidden_state.shap...  58.4 us
    all_to_all x1, waiting for transfers between devices, shards(): lax.all_to_all(answers, 'ep', split_axis=0, concat_axis=0, tiled=True)  29.4 us
    all_to_all x1, blocking collectives, copy_for_each(): lax.all_to_all(jnp.broadcast_to(array[None], (length, *array.shape)), axi...  7.54 us
    all_to_all x1, starting transfers between devices, shards(): lax.all_to_all(answers, 'ep', split_axis=0, concat_axis=0, tiled=True)  7.18 us
    dot_general x1, matrix products, expert_rows(): jnp.dot(activated, down_matrix[0], preferred_element_type=jnp.float32)  6.21 us
    psum x1, blocking collectives, shards(): total_squares = lax.psum(local_squares, 'tp')  4.96 us
    all_to_all x1, blocking collectives, sum_at_owner(): lax.all_to_all(in_blocks(array, dim, length), axis, 0, 0, tiled=True)  4.58 us
    dot_general x1, matrix products, expert_rows(): jnp.dot(token_rows, gate_matrix[0], preferred_element_type=jnp.float32)  2.62 us
  transfers between devices with their start and end apart: 1, of which 1 were waited for; matrix products, arithmetic and copies ran while one was open for 0% of the time, Pallas kernels for 0%

commit v1 on v0

v1 whole, which is shorter than its diff:
```python
import functools

import jax
import jax.numpy as jnp
from jax import lax
from jax.experimental import pallas as pl
from jax.experimental.pallas import tpu as pltpu
from jax.sharding import PartitionSpec as P

MESH = pl.DeviceIdType.MESH
norm_eps = 1e-05
COLUMNS = 4
STRIDE = 4
SLOTS = COLUMNS * STRIDE
SELF = SLOTS - 1
SOURCE = (0, -STRIDE, STRIDE, 2 * STRIDE)
LANES = 128


def window(slot):
    number = (slot + 5) % SLOTS
    row, column = number // COLUMNS, number % COLUMNS
    return row - 1 - column % 2, column


def kernel(
    planes,
    h_ref, meta_ref, gain_ref, gate_ref, up_ref, down_ref,
    out_ref,
    gate_w, up_w, down_w, blocks, metas, outgoing, mine, other, act, part_out, part_in, own_part,
    answers, returned, weight_hi, weight_lo, near_sum, travel, chain_in, final_in, square_out, square_in,
    w_sem, m_send, m_recv, h_send, h_recv, d_send, d_recv, x_send, x_recv, s_send, s_recv, r_send, r_recv,
    c_send, c_recv, f_send, f_recv, q_send, q_recv,
):
    tokens, width = h_ref.shape
    capacity = outgoing.shape[2]
    rows = SLOTS * capacity
    half = tokens // 2
    top = meta_ref.shape[0] // 2
    core = lax.axis_index("tp")
    me = lax.axis_index("ep")
    plane, column = me // COLUMNS, lax.rem(me, COLUMNS)

    def at(planes_on, columns_on):
        return lax.rem(plane + planes_on + planes, planes) * COLUMNS + lax.rem(
            column + columns_on + COLUMNS, COLUMNS
        )

    def remote(src, dst, send, recv, where):
        return pltpu.make_async_remote_copy(
            src_ref=src, dst_ref=dst, send_sem=send, recv_sem=recv, device_id=where, device_id_type=MESH
        )

    partner = {"tp": 1 - core}

    loads = []
    for side in range(2):
        at_core = (core + side) % 2
        span = pl.ds(pl.multiple_of(at_core * width, width), width)
        for order, (source, target) in enumerate(
            (
                (gate_ref.at[0, span, :], gate_w.at[pl.ds(side * width, width), :]),
                (up_ref.at[0, span, :], up_w.at[pl.ds(side * width, width), :]),
                (down_ref.at[0, :, span], down_w.at[side]),
            )
        ):
            load = pltpu.make_async_copy(source, target, w_sem.at[side * 3 + order])
            load.start()
            loads.append(load)

    greeted = {(STRIDE, 0), (-STRIDE, 0)}
    for slot in range(SLOTS - 1):
        planes_on, columns_on = window(slot)
        greeted.add((planes_on, columns_on))
        greeted.add((-planes_on, (-columns_on) % COLUMNS))
    barrier = pltpu.get_barrier_semaphore()
    for planes_on, columns_on in sorted(greeted):
        pl.semaphore_signal(barrier, inc=1, device_id={"ep": at(planes_on, columns_on)}, device_id_type=MESH)
    pl.semaphore_signal(barrier, inc=1, device_id=partner, device_id_type=MESH)

    row_at = lax.broadcasted_iota(jnp.int32, (rows, LANES), 0)
    number = lax.rem(row_at // capacity + 5, SLOTS)
    row_column = lax.rem(number, COLUMNS)
    row_plane = lax.rem(plane + number // COLUMNS - 1 - lax.rem(row_column, 2) + planes, planes)
    row_expert = (row_plane * COLUMNS + lax.rem(column + row_column, COLUMNS)).astype(jnp.float32)
    row_slot = lax.rem(row_at, capacity).astype(jnp.float32)
    before = (
        lax.broadcasted_iota(jnp.int32, (LANES, LANES), 0) < lax.broadcasted_iota(jnp.int32, (LANES, LANES), 1)
    ).astype(jnp.bfloat16)

    def place(b):
        meta = meta_ref if b == 0 else metas.at[b - 1]
        named = jnp.zeros((rows, LANES), jnp.float32)
        weight = jnp.zeros((rows, LANES), jnp.float32)
        for k in range(top):
            match = meta[k : k + 1, :] == row_expert
            named = named + jnp.where(match, 1.0, 0.0)
            weight = weight + jnp.where(match, meta[top + k : top + k + 1, :], 0.0)
        rank = jnp.dot(named.astype(jnp.bfloat16), before, preferred_element_type=jnp.float32)
        placed = jnp.where(rank == row_slot, named, 0.0)
        block = h_ref[...] if b == 0 else blocks[b - 1]
        chosen = jnp.dot(placed[:, :tokens].astype(jnp.bfloat16), block, preferred_element_type=jnp.float32)
        outgoing[b] = chosen.reshape(SLOTS, capacity, width).astype(jnp.bfloat16)
        weights = (placed * weight).T[:tokens]
        high = weights.astype(jnp.bfloat16)
        weight_hi[b] = high
        weight_lo[b] = (weights - high.astype(jnp.float32)).astype(jnp.bfloat16)

    def send_slots(b, source, target, send, recv, sign):
        for slot in range(SLOTS - 1):
            planes_on, columns_on = window(slot)
            remote(
                source.at[b, slot],
                target.at[b, slot],
                send.at[b],
                recv.at[b],
                {"ep": at(sign * planes_on, sign * columns_on)},
            ).start()
        target[b, SELF] = source[b, SELF]

    def wait_slots(b, buffer, sem):
        span = buffer.at[b, pl.ds(0, SLOTS - 1)]
        pltpu.make_async_copy(span, span, sem.at[b]).wait()

    place(0)
    pl.semaphore_wait(barrier, len(greeted) + 1)

    up_ring, down_ring = {"ep": at(STRIDE, 0)}, {"ep": at(-STRIDE, 0)}
    spans = (pl.ds(0, half), pl.ds(half, half))
    first = []

    def go(copy):
        copy.start()
        first.append(copy)
        return copy

    def block_to(b, source, where, part):
        return go(
            remote(
                source.at[spans[part]],
                blocks.at[b - 1, spans[part]],
                h_send.at[b - 1, part],
                h_recv.at[b - 1, part],
                where,
            )
        )

    meta_up = go(remote(meta_ref, metas.at[0], m_send.at[0], m_recv.at[0], up_ring))
    meta_down = go(remote(meta_ref, metas.at[1], m_send.at[1], m_recv.at[1], down_ring))
    up_low = block_to(1, h_ref, up_ring, 0)
    down_high = block_to(2, h_ref, down_ring, 1)
    up_high = block_to(1, h_ref, up_ring, 1)
    down_low = block_to(2, h_ref, down_ring, 0)
    send_slots(0, outgoing, mine, d_send, d_recv, 1)

    meta_up.wait_recv()
    meta_far = go(remote(metas.at[0], metas.at[2], m_send.at[2], m_recv.at[2], up_ring))
    up_low.wait_recv()
    far_low = block_to(3, blocks.at[0], up_ring, 0)
    down_high.wait_recv()
    far_high = block_to(3, blocks.at[1], down_ring, 1)
    up_high.wait_recv()
    place(1)
    send_slots(1, outgoing, mine, d_send, d_recv, 1)
    meta_down.wait_recv()
    down_low.wait_recv()
    place(2)
    send_slots(2, outgoing, mine, d_send, d_recv, 1)

    def exchange(group):
        for b in group:
            wait_slots(b, mine, d_recv)
        span = pl.ds(group[0], len(group))
        copy = remote(mine.at[span], other.at[span], x_send.at[group[0]], x_recv.at[group[0]], partner)
        return go(copy)

    def experts(group, swap):
        count = len(group) * rows
        span = pl.ds(group[0], len(group))
        swap.wait_recv()
        tokens_in = jnp.concatenate(
            [mine[span].reshape(count, width), other[span].reshape(count, width)], axis=1
        )
        step = 256
        for start in range(0, gate_w.shape[1], step):
            gate = jnp.dot(tokens_in, gate_w[:, start : start + step], preferred_element_type=jnp.float32)
            up = jnp.dot(tokens_in, up_w[:, start : start + step], preferred_element_type=jnp.float32)
            value = gate * (1.0 / (1.0 + jnp.exp(-gate))) * up
            act[pl.ds(0, count), start : start + step] = value.astype(jnp.bfloat16)
        active = act[pl.ds(0, count), :]
        away = jnp.dot(active, down_w[1], preferred_element_type=jnp.float32)
        part_out[span] = away.astype(jnp.bfloat16).reshape(len(group), rows, width)
        copy = go(remote(part_out.at[span], part_in.at[span], s_send.at[group[0]], s_recv.at[group[0]], partner))
        here = jnp.dot(active, down_w[0], preferred_element_type=jnp.float32)
        own_part[span] = here.astype(jnp.bfloat16).reshape(len(group), rows, width)
        return copy

    def answer(group, copy):
        copy.wait_recv()
        for b in group:
            both = own_part[b].astype(jnp.float32) + part_in[b].astype(jnp.float32)
            answers[b] = both.reshape(SLOTS, capacity, width).astype(jnp.bfloat16)
            send_slots(b, answers, returned, r_send, r_recv, -1)

    def combine(b):
        wait_slots(b, returned, r_recv)
        slots = returned[b].reshape(rows, width)
        return jnp.dot(weight_hi[b], slots, preferred_element_type=jnp.float32) + jnp.dot(
            weight_lo[b], slots, preferred_element_type=jnp.float32
        )

    swap = exchange((0,))
    for load in loads:
        load.wait()
    part = experts((0,), swap)

    far_low.wait_recv()
    far_high.wait_recv()
    meta_far.wait_recv()
    place(3)
    send_slots(3, outgoing, mine, d_send, d_recv, 1)

    answer((0,), part)
    swap = exchange((1, 2))
    part = experts((1, 2), swap)
    swap = exchange((3,))
    answer((1, 2), part)
    part = experts((3,), swap)
    answer((3,), part)

    near_sum[0] = combine(0)
    near = combine(1)
    near_sum[1] = near
    travel[0] = near.astype(jnp.bfloat16)
    finals = {}

    def final_to(b, where, part):
        finals[b, part] = go(
            remote(
                travel.at[b - 1, spans[part]],
                final_in.at[b - 1, spans[part]],
                f_send.at[b - 1, part],
                f_recv.at[b - 1, part],
                where,
            )
        )

    final_to(1, down_ring, 1)
    near = combine(2)
    near_sum[2] = near
    travel[1] = near.astype(jnp.bfloat16)
    final_to(2, up_ring, 0)
    travel[2] = combine(3).astype(jnp.bfloat16)
    chains = []
    for part_at, where in ((0, down_ring), (1, up_ring)):
        chains.append(
            go(
                remote(
                    travel.at[2, spans[part_at]],
                    chain_in.at[spans[part_at]],
                    c_send.at[part_at],
                    c_recv.at[part_at],
                    where,
                )
            )
        )
    for part_at, (b, where) in enumerate(((1, down_ring), (2, up_ring))):
        chains[part_at].wait_recv()
        total = near_sum[b, spans[part_at]] + chain_in[spans[part_at]].astype(jnp.float32)
        travel[b - 1, spans[part_at]] = total.astype(jnp.bfloat16)
        final_to(b, where, part_at)
    for copy in finals.values():
        copy.wait_recv()
    combined = near_sum[0] + final_in[0].astype(jnp.float32) + final_in[1].astype(jnp.float32)
    squares = jnp.sum(combined * combined, axis=1, keepdims=True)
    square_out[...] = jnp.broadcast_to(squares, square_out.shape)
    copy = go(remote(square_out, square_in, q_send.at[0], q_recv.at[0], partner))
    copy.wait_recv()
    mean = (squares + square_in[:, :1]) / (2 * width)
    out_ref[...] = (combined * lax.rsqrt(mean + norm_eps) * gain_ref[...]).astype(jnp.bfloat16)

    for copy in first:
        copy.wait_send()
    for b in range(len(SOURCE)):
        wait_slots(b, outgoing, d_send)
        wait_slots(b, answers, r_send)


def solution(mesh):
    experts = mesh.shape["ep"]
    planes = experts // COLUMNS
    assert planes == STRIDE * len(SOURCE) and mesh.shape["tp"] == 2

    def shards(hidden_state, expert_ids, route_weight, gate_matrix, up_matrix, down_matrix, norm_gain):
        tokens, top = expert_ids.shape
        width = hidden_state.shape[1]
        hidden = gate_matrix.shape[2]
        capacity = max(2, 2 * tokens * top // experts)
        rows = SLOTS * capacity
        count = len(SOURCE)
        spare = ((0, 0), (0, LANES - tokens))
        meta = jnp.concatenate(
            [
                jnp.pad(expert_ids.T.astype(jnp.float32), spare, constant_values=-1.0),
                jnp.pad(route_weight.T, spare),
            ]
        )
        vmem, anywhere = pl.BlockSpec(memory_space=pltpu.VMEM), pl.BlockSpec(memory_space=pl.ANY)
        slots = pltpu.VMEM((count, SLOTS, capacity, width), jnp.bfloat16)
        parts = pltpu.VMEM((count, rows, width), jnp.bfloat16)
        dma = pltpu.SemaphoreType.DMA
        return pl.pallas_call(
            functools.partial(kernel, planes),
            out_shape=jax.ShapeDtypeStruct((tokens, width), jnp.bfloat16),
            in_specs=[vmem, vmem, vmem, anywhere, anywhere, anywhere],
            out_specs=vmem,
            scratch_shapes=[
                pltpu.VMEM((2 * width, hidden), jnp.bfloat16),
                pltpu.VMEM((2 * width, hidden), jnp.bfloat16),
                pltpu.VMEM((2, hidden, width), jnp.bfloat16),
                pltpu.VMEM((count - 1, tokens, width), jnp.bfloat16),
                pltpu.VMEM((count - 1, 2 * top, LANES), jnp.float32),
                slots,
                slots,
                slots,
                pltpu.VMEM((2 * rows, hidden), jnp.bfloat16),
                parts,
                parts,
                parts,
                slots,
                slots,
                pltpu.VMEM((count, tokens, rows), jnp.bfloat16),
                pltpu.VMEM((count, tokens, rows), jnp.bfloat16),
                pltpu.VMEM((3, tokens, width), jnp.float32),
                pltpu.VMEM((3, tokens, width), jnp.bfloat16),
                pltpu.VMEM((tokens, width), jnp.bfloat16),
                pltpu.VMEM((2, tokens, width), jnp.bfloat16),
                pltpu.VMEM((tokens, LANES), jnp.float32),
                pltpu.VMEM((tokens, LANES), jnp.float32),
                dma((6,)),
                dma((3,)), dma((3,)),
                dma((3, 2)), dma((3, 2)),
                dma((count,)), dma((count,)),
                dma((count,)), dma((count,)),
                dma((count,)), dma((count,)),
                dma((count,)), dma((count,)),
                dma((2,)), dma((2,)),
                dma((2, 2)), dma((2, 2)),
                dma((1,)), dma((1,)),
            ],
            compiler_params=pltpu.CompilerParams(
                collective_id=0, has_side_effects=True, vmem_limit_bytes=48 * 1024 * 1024
            ),
        )(hidden_state, meta, norm_gain.reshape(1, width), gate_matrix, up_matrix, down_matrix)

    placed = (
        P(("grp", "ep"), "tp"),
        P(("grp", "ep"), None),
        P(("grp", "ep"), None),
        P("ep", None, "tp"),
        P("ep", None, "tp"),
        P("ep", "tp", None),
        P("tp"),
    )
    return jax.shard_map(
        shards, mesh=mesh, in_specs=placed, out_specs=P(("grp", "ep"), "tp"), check_vma=False
    )
```

time: 131 us -> 76.9 us (0.59)
  blocking collectives: 75.4 us -> 0 us
  Pallas kernels: 0 us -> 69.9 us
  waiting for transfers between devices: 29.4 us -> 0 us
  matrix products: 10.5 us -> 0 us
  starting transfers between devices: 7.18 us -> 0 us
  other arithmetic: 3.66 us -> 1.37 us
    all_to_all x3 -> x0, blocking collectives: 70.5 us -> none  [the longest x1 58.4 us: shards(): lax.all_to_all(outgoing.reshape(expert_count, capacity, hidden_state.shap...]
    pallas_call x0 -> x1, Pallas kernels: none -> 69.9 us  [shards(): pl.pallas_call(functools.partial(kernel, planes), out_shape=jax.ShapeDtyp...]
    all_to_all x1 -> x0, waiting for transfers between devices: 29.4 us -> none  [shards(): lax.all_to_all(answers, 'ep', split_axis=0, concat_axis=0, tiled=True)]
    dot_general x4 -> x0, matrix products: 10.5 us -> none  [the longest x1 6.21 us: expert_rows(): jnp.dot(activated, down_matrix[0], preferred_element_type=jnp.float32)]
    all_to_all x1 -> x0, starting transfers between devices: 7.18 us -> none  [shards(): lax.all_to_all(answers, 'ep', split_axis=0, concat_axis=0, tiled=True)]
    psum x1 -> x0, blocking collectives: 4.96 us -> none  [shards(): total_squares = lax.psum(local_squares, 'tp')]
    unnamed x8 -> x9, local copies, waits for them, and re-layouts: 1.18 us -> 5.33 us
    reshape x4 -> x0, local copies, waits for them, and re-layouts: 1.48 us -> none  [the longest x1 1.3 us: in_blocks(): return jnp.moveaxis(array.reshape(*before, length, -1, *after), dim, 0)]
  transfers between devices with their start and end apart: 1 -> 0, of which waited for: 1 -> 0; matrix products, arithmetic and copies ran while one was open for 0% -> 0% of each run, Pallas kernels for 0% -> 0%
where the time goes in v1:
time: 76.9 us; the launch traced here: 76.6 us
  Pallas kernels  69.9 us (91%)
  local copies, waits for them, and re-layouts  5.33 us (7%)
  other arithmetic  1.37 us (2%)
    pallas_call x1, Pallas kernels, shards(): pl.pallas_call(functools.partial(kernel, planes), out_shape=jax.ShapeDtyp...  69.9 us
    unnamed x9, local copies, waits for them, and re-layouts  5.33 us

profile of v1, /device:TPU:33, one launch (start us, length us, event | category | flops | bytes accessed | tf_op | source)
XLA Modules:
  0.0 76.6 jit_solution(6222934164916158264)
XLA Ops:
  0.0 0.7 convert_bitcast_fusion
  0.7 0.7 select_maximum_fusion.meta_ref
  1.4 0.0 copy-start
  1.4 1.6 %copy-done = bf16[1,1024,1024]{2,1,0:T(8,128)(2,1)S(1)} copy-done((bf16[1,1024,1024]{2,1,0:T(8,128)(2,1)S(1)}, bf16[1,1024,1024]{2,1,0:T(8,128)(2,1)}, u32[]{:S(2)}) %copy-start) | copy-done | bytes 2097176
  3.0 0.0 copy-start.1
  3.0 1.6 %copy-done.1 = bf16[1,1024,1024]{2,1,0:T(8,128)(2,1)S(1)} copy-done((bf16[1,1024,1024]{2,1,0:T(8,128)(2,1)S(1)}, bf16[1,1024,1024]{2,1,0:T(8,128)(2,1)}, u32[]{:S(2)}) %copy-start.1) | copy-done | bytes 2097176
  4.6 0.0 copy-start.2
  4.6 0.8 %copy-done.2 = bf16[64,512]{1,0:T(8,128)(2,1)S(1)} copy-done((bf16[64,512]{1,0:T(8,128)(2,1)S(1)}, bf16[64,512]{1,0:T(8,128)(2,1)}, u32[]{:S(2)}) %copy-start.2) | copy-done | bytes 65560
  5.4 0.0 copy-start.3
  5.4 0.7 copy-done.3
  6.1 69.9 %shard_map.73 = bf16[64,512]{1,0:T(8,128)(2,1)S(1)} custom-call(bf16[64,512]{1,0:T(8,128)(2,1)S(1)} %copy-done.2, f32[8,128]{1,0:T(8,128)S(1)} %select_maximum_fusion.meta_ref, f32[1,512]{1,0:T(1,128)S(1)} %bitcast.4, bf16[1,1024,1024]{2,1,0:T(8,128)(2,1)S(1)} %copy-done, bf16[1,1024,1024]{2,1,0:T(8,128)(2,1)S(1)} %copy-done.1, bf16[1,1024,1024]{2,1,0:T(8,128)(2,1)} %down_ref.1), custom_call_target="tpu_custom_call" | custom-call | tf_op jit(solution)/shard_map/pallas_call | solution.py:312
  76.0 0.6 copy.9
Async XLA Ops:
  1.4 1.6 %copy-start = (bf16[1,1024,1024]{2,1,0:T(8,128)(2,1)S(1)}, bf16[1,1024,1024]{2,1,0:T(8,128)(2,1)}, u32[]{:S(2)}) copy-start(bf16[1,1024,1024]{2,1,0:T(8,128)(2,1)} %gate_ref.1) | copy-start | bytes 6291460
  3.0 1.6 %copy-start.1 = (bf16[1,1024,1024]{2,1,0:T(8,128)(2,1)S(1)}, bf16[1,1024,1024]{2,1,0:T(8,128)(2,1)}, u32[]{:S(2)}) copy-start(bf16[1,1024,1024]{2,1,0:T(8,128)(2,1)} %up_ref.1) | copy-start | bytes 6291460
  4.6 0.8 %copy-start.2 = (bf16[64,512]{1,0:T(8,128)(2,1)S(1)}, bf16[64,512]{1,0:T(8,128)(2,1)}, u32[]{:S(2)}) copy-start(bf16[64,512]{1,0:T(8,128)(2,1)} %h_ref.1) | copy-start | bytes 196612
  5.4 0.7 copy-start.3

commit v2 on v1

--- a/solution.py
+++ b/solution.py
@@ -15,6 +15,7 @@
 SELF = SLOTS - 1
 SOURCE = (0, -STRIDE, STRIDE, 2 * STRIDE)
 LANES = 128
+CHUNKS = 2
 
 
 def window(slot):
@@ -25,18 +26,25 @@
 
 def kernel(
     planes,
-    h_ref, meta_ref, gain_ref, gate_ref, up_ref, down_ref,
+    h_hbm, ids_hbm, route_hbm, gain_hbm, gate_ref, up_ref, down_ref,
     out_ref,
-    gate_w, up_w, down_w, blocks, metas, outgoing, mine, other, act, part_out, part_in, own_part,
+    h_ref, ids_ref, route_ref, gain_ref, meta_ref, gate_w, up_w, down_w, blocks, metas, outgoing, mine, other, act, part_out, part_in, own_part,
     answers, returned, weight_hi, weight_lo, near_sum, travel, chain_in, final_in, square_out, square_in,
-    w_sem, m_send, m_recv, h_send, h_recv, d_send, d_recv, x_send, x_recv, s_send, s_recv, r_send, r_recv,
+    i_sem, w_sem, m_send, m_recv, h_send, h_recv, d_send, d_recv, x_send, x_recv, s_send, s_recv, r_send, r_recv,
     c_send, c_recv, f_send, f_recv, q_send, q_recv,
 ):
     tokens, width = h_ref.shape
     capacity = outgoing.shape[2]
     rows = SLOTS * capacity
     half = tokens // 2
-    top = meta_ref.shape[0] // 2
+    top = ids_ref.shape[0]
+    inputs = []
+    for order, (source, target) in enumerate(
+        ((ids_hbm, ids_ref), (route_hbm, route_ref), (h_hbm, h_ref), (gain_hbm, gain_ref))
+    ):
+        load = pltpu.make_async_copy(source, target, i_sem.at[order])
+        load.start()
+        inputs.append(load)
     core = lax.axis_index("tp")
     me = lax.axis_index("ep")
     plane, column = me // COLUMNS, lax.rem(me, COLUMNS)
@@ -52,21 +60,6 @@
         )
 
     partner = {"tp": 1 - core}
-
-    loads = []
-    for side in range(2):
-        at_core = (core + side) % 2
-        span = pl.ds(pl.multiple_of(at_core * width, width), width)
-        for order, (source, target) in enumerate(
-            (
-                (gate_ref.at[0, span, :], gate_w.at[pl.ds(side * width, width), :]),
-                (up_ref.at[0, span, :], up_w.at[pl.ds(side * width, width), :]),
-                (down_ref.at[0, :, span], down_w.at[side]),
-            )
-        ):
-            load = pltpu.make_async_copy(source, target, w_sem.at[side * 3 + order])
-            load.start()
-            loads.append(load)
 
     greeted = {(STRIDE, 0), (-STRIDE, 0)}
     for slot in range(SLOTS - 1):
@@ -122,10 +115,33 @@
         span = buffer.at[b, pl.ds(0, SLOTS - 1)]
         pltpu.make_async_copy(span, span, sem.at[b]).wait()
 
+    for load in inputs:
+        load.wait()
+    loads = []
+    for side in range(2):
+        at_core = (core + side) % 2
+        span = pl.ds(pl.multiple_of(at_core * width, width), width)
+        for order, (source, target) in enumerate(
+            (
+                (gate_ref.at[0, span, :], gate_w.at[pl.ds(side * width, width), :]),
+                (up_ref.at[0, span, :], up_w.at[pl.ds(side * width, width), :]),
+                (down_ref.at[0, :, span], down_w.at[side]),
+            )
+        ):
+            load = pltpu.make_async_copy(source, target, w_sem.at[side * 3 + order])
+            load.start()
+            loads.append(load)
+
+    meta_ref[...] = jnp.full(meta_ref.shape, -1.0, jnp.float32)
+    meta_ref[0:top, 0:tokens] = ids_ref[...].astype(jnp.float32)
+    meta_ref[top : 2 * top, 0:tokens] = route_ref[...]
     place(0)
     pl.semaphore_wait(barrier, len(greeted) + 1)
 
     up_ring, down_ring = {"ep": at(STRIDE, 0)}, {"ep": at(-STRIDE, 0)}
+    quarter = half // CHUNKS
+    chunks = [pl.ds(part * quarter, quarter) for part in range(2 * CHUNKS)]
+    relayed = (range(CHUNKS), range(CHUNKS, 2 * CHUNKS))
     spans = (pl.ds(0, half), pl.ds(half, half))
     first = []
 
@@ -134,38 +150,43 @@
         first.append(copy)
         return copy
 
-    def block_to(b, source, where, part):
+    def block_to(b, source, where, rows_in, sem):
         return go(
             remote(
-                source.at[spans[part]],
-                blocks.at[b - 1, spans[part]],
-                h_send.at[b - 1, part],
-                h_recv.at[b - 1, part],
+                source.at[rows_in],
+                blocks.at[b - 1, rows_in],
+                h_send.at[b - 1, sem],
+                h_recv.at[b - 1, sem],
                 where,
             )
         )
 
-    meta_up = go(remote(meta_ref, metas.at[0], m_send.at[0], m_recv.at[0], up_ring))
-    meta_down = go(remote(meta_ref, metas.at[1], m_send.at[1], m_recv.at[1], down_ring))
-    up_low = block_to(1, h_ref, up_ring, 0)
-    down_high = block_to(2, h_ref, down_ring, 1)
-    up_high = block_to(1, h_ref, up_ring, 1)
-    down_low = block_to(2, h_ref, down_ring, 0)
+    ways = (up_ring, down_ring)
+    meta_near = [
+        go(remote(meta_ref, metas.at[way], m_send.at[way], m_recv.at[way], where)) for way, where in enumerate(ways)
+    ]
+    relay = {}
+    for step in range(CHUNKS):
+        for way, where in enumerate(ways):
+            part = relayed[way][step]
+            relay[way, part] = block_to(1 + way, h_ref, where, chunks[part], part)
+    near = [block_to(1 + way, h_ref, where, spans[1 - way], relayed[1 - way][0]) for way, where in enumerate(ways)]
     send_slots(0, outgoing, mine, d_send, d_recv, 1)
 
-    meta_up.wait_recv()
-    meta_far = go(remote(metas.at[0], metas.at[2], m_send.at[2], m_recv.at[2], up_ring))
-    up_low.wait_recv()
-    far_low = block_to(3, blocks.at[0], up_ring, 0)
-    down_high.wait_recv()
-    far_high = block_to(3, blocks.at[1], down_ring, 1)
-    up_high.wait_recv()
-    place(1)
-    send_slots(1, outgoing, mine, d_send, d_recv, 1)
-    meta_down.wait_recv()
-    down_low.wait_recv()
-    place(2)
-    send_slots(2, outgoing, mine, d_send, d_recv, 1)
+    far = []
+    for step in range(CHUNKS):
+        for way, where in enumerate(ways):
+            part = relayed[way][step]
+            relay[way, part].wait_recv()
+            far.append(block_to(3, blocks.at[way], where, chunks[part], part))
+        if step == 0:
+            meta_near[0].wait_recv()
+            far.append(go(remote(metas.at[0], metas.at[2], m_send.at[2], m_recv.at[2], up_ring)))
+    meta_near[1].wait_recv()
+    for way in range(2):
+        near[way].wait_recv()
+        place(1 + way)
+        send_slots(1 + way, outgoing, mine, d_send, d_recv, 1)
 
     def exchange(group):
         for b in group:
@@ -209,67 +230,61 @@
             weight_lo[b], slots, preferred_element_type=jnp.float32
         )
 
-    swap = exchange((0,))
+    for copy in far:
+        copy.wait_recv()
+    place(3)
+    send_slots(3, outgoing, mine, d_send, d_recv, 1)
+
     for load in loads:
         load.wait()
-    part = experts((0,), swap)
-
-    far_low.wait_recv()
-    far_high.wait_recv()
-    meta_far.wait_recv()
-    place(3)
-    send_slots(3, outgoing, mine, d_send, d_recv, 1)
-
-    answer((0,), part)
-    swap = exchange((1, 2))
-    part = experts((1, 2), swap)
-    swap = exchange((3,))
-    answer((1, 2), part)
-    part = experts((3,), swap)
-    answer((3,), part)
-
-    near_sum[0] = combine(0)
-    near = combine(1)
-    near_sum[1] = near
-    travel[0] = near.astype(jnp.bfloat16)
-    finals = {}
-
-    def final_to(b, where, part):
-        finals[b, part] = go(
-            remote(
-                travel.at[b - 1, spans[part]],
-                final_in.at[b - 1, spans[part]],
-                f_send.at[b - 1, part],
-                f_recv.at[b - 1, part],
-                where,
+    part_own = experts((0,), exchange((0,)))
+    swap_near = [exchange((b,)) for b in (1, 2)]
+    swap_far = exchange((3,))
+    part_up = experts((1,), swap_near[0])
+    part_far = experts((3,), swap_far)
+    answer((0,), part_own)
+    part_down = experts((2,), swap_near[1])
+    answer((3,), part_far)
+    answer((1,), part_up)
+    answer((2,), part_down)
+
+    travel[2] = combine(3).astype(jnp.bfloat16)
+    back = (down_ring, up_ring)
+    chains, finals = {}, []
+    for step in range(CHUNKS):
+        for way, where in enumerate(back):
+            part = relayed[way][step]
+            chains[way, part] = go(
+                remote(travel.at[2, chunks[part]], chain_in.at[chunks[part]], c_send.at[part], c_recv.at[part], where)
             )
-        )
-
-    final_to(1, down_ring, 1)
-    near = combine(2)
-    near_sum[2] = near
-    travel[1] = near.astype(jnp.bfloat16)
-    final_to(2, up_ring, 0)
-    travel[2] = combine(3).astype(jnp.bfloat16)
-    chains = []
-    for part_at, where in ((0, down_ring), (1, up_ring)):
-        chains.append(
+    for b in range(3):
+        near_sum[b] = combine(b)
+
+    def final_to(way, rows_in, sem):
+        finals.append(
             go(
                 remote(
-                    travel.at[2, spans[part_at]],
-                    chain_in.at[spans[part_at]],
-                    c_send.at[part_at],
-                    c_recv.at[part_at],
-                    where,
+                    travel.at[way, rows_in],
+                    final_in.at[way, rows_in],
+                    f_send.at[way, sem],
+                    f_recv.at[way, sem],
+                    back[way],
                 )
             )
         )
-    for part_at, (b, where) in enumerate(((1, down_ring), (2, up_ring))):
-        chains[part_at].wait_recv()
-        total = near_sum[b, spans[part_at]] + chain_in[spans[part_at]].astype(jnp.float32)
-        travel[b - 1, spans[part_at]] = total.astype(jnp.bfloat16)
-        final_to(b, where, part_at)
-    for copy in finals.values():
+
+    for way in range(2):
+        rows_in = spans[1 - way]
+        travel[way, rows_in] = near_sum[1 + way, rows_in].astype(jnp.bfloat16)
+        final_to(way, rows_in, relayed[1 - way][0])
+    for step in range(CHUNKS):
+        for way in range(2):
+            part = relayed[way][step]
+            chains[way, part].wait_recv()
+            total = near_sum[1 + way, chunks[part]] + chain_in[chunks[part]].astype(jnp.float32)
+            travel[way, chunks[part]] = total.astype(jnp.bfloat16)
+            final_to(way, chunks[part], part)
+    for copy in finals:
         copy.wait_recv()
     combined = near_sum[0] + final_in[0].astype(jnp.float32) + final_in[1].astype(jnp.float32)
     squares = jnp.sum(combined * combined, axis=1, keepdims=True)
@@ -298,23 +313,21 @@
         capacity = max(2, 2 * tokens * top // experts)
         rows = SLOTS * capacity
         count = len(SOURCE)
-        spare = ((0, 0), (0, LANES - tokens))
-        meta = jnp.concatenate(
-            [
-                jnp.pad(expert_ids.T.astype(jnp.float32), spare, constant_values=-1.0),
-                jnp.pad(route_weight.T, spare),
-            ]
-        )
-        vmem, anywhere = pl.BlockSpec(memory_space=pltpu.VMEM), pl.BlockSpec(memory_space=pl.ANY)
+        vmem, hbm = pl.BlockSpec(memory_space=pltpu.VMEM), pl.BlockSpec(memory_space=pltpu.HBM)
         slots = pltpu.VMEM((count, SLOTS, capacity, width), jnp.bfloat16)
         parts = pltpu.VMEM((count, rows, width), jnp.bfloat16)
         dma = pltpu.SemaphoreType.DMA
         return pl.pallas_call(
             functools.partial(kernel, planes),
-            out_shape=jax.ShapeDtypeStruct((tokens, width), jnp.bfloat16),
-            in_specs=[vmem, vmem, vmem, anywhere, anywhere, anywhere],
+            out_shape=pltpu.VMEM((tokens, width), jnp.bfloat16),
+            in_specs=[hbm] * 7,
             out_specs=vmem,
             scratch_shapes=[
+                pltpu.VMEM((tokens, width), jnp.bfloat16),
+                pltpu.VMEM((top, tokens), jnp.int32),
+                pltpu.VMEM((top, tokens), jnp.float32),
+                pltpu.VMEM((1, width), jnp.float32),
+                pltpu.VMEM((2 * top, LANES), jnp.float32),
                 pltpu.VMEM((2 * width, hidden), jnp.bfloat16),
                 pltpu.VMEM((2 * width, hidden), jnp.bfloat16),
                 pltpu.VMEM((2, hidden, width), jnp.bfloat16),
@@ -337,21 +350,22 @@
                 pltpu.VMEM((2, tokens, width), jnp.bfloat16),
                 pltpu.VMEM((tokens, LANES), jnp.float32),
                 pltpu.VMEM((tokens, LANES), jnp.float32),
+                dma((4,)),
                 dma((6,)),
                 dma((3,)), dma((3,)),
-                dma((3, 2)), dma((3, 2)),
+                dma((3, 2 * CHUNKS)), dma((3, 2 * CHUNKS)),
                 dma((count,)), dma((count,)),
                 dma((count,)), dma((count,)),
                 dma((count,)), dma((count,)),
                 dma((count,)), dma((count,)),
-                dma((2,)), dma((2,)),
-                dma((2, 2)), dma((2, 2)),
+                dma((2 * CHUNKS,)), dma((2 * CHUNKS,)),
+                dma((2, 2 * CHUNKS)), dma((2, 2 * CHUNKS)),
                 dma((1,)), dma((1,)),
             ],
             compiler_params=pltpu.CompilerParams(
-                collective_id=0, has_side_effects=True, vmem_limit_bytes=48 * 1024 * 1024
+                collective_id=0, has_side_effects=True, vmem_limit_bytes=64_000_000
             ),
-        )(hidden_state, meta, norm_gain.reshape(1, width), gate_matrix, up_matrix, down_matrix)
+        )(hidden_state, expert_ids.T, route_weight.T, norm_gain.reshape(1, width), gate_matrix, up_matrix, down_matrix)
 
     placed = (
         P(("grp", "ep"), "tp"),

time: 76.9 us -> 70.6 us (0.918)
  local copies, waits for them, and re-layouts: 5.33 us -> 0.63 us
  other arithmetic: 1.37 us -> 0 us
    unnamed x9 -> x1, local copies, waits for them, and re-layouts: 5.33 us -> 0.63 us
where the time goes in v2:
time: 70.6 us; the launch traced here: 70.4 us
  Pallas kernels  69.8 us (99%)
    pallas_call x1, Pallas kernels, shards(): pl.pallas_call(functools.partial(kernel, planes), out_shape=pltpu.VMEM((t...  69.8 us

profile of v2, /device:TPU:33, one launch (start us, length us, event | category | flops | bytes accessed | tf_op | source)
XLA Modules:
  0.0 70.4 jit_solution(3694656371080860226)
XLA Ops:
  0.0 69.8 %shard_map.73 = bf16[64,512]{1,0:T(8,128)(2,1)S(1)} custom-call(bf16[64,512]{1,0:T(8,128)(2,1)} %h_hbm.1, s32[4,64]{1,0:T(4,128)} %bitcast.3, f32[4,64]{1,0:T(4,128)} %bitcast.4, f32[1,512]{1,0:T(1,128)} %bitcast.5, bf16[1,1024,1024]{2,1,0:T(8,128)(2,1)} %gate_ref.1, bf16[1,1024,1024]{2,1,0:T(8,128)(2,1)} %up_ref.1, bf16[1,1024,1024]{2,1,0:T(8,128)(2,1)} %down_ref.1), custom_call_target="tpu_custom_call" | custom-call | tf_op jit(solution)/shard_map/pallas_call | solution.py:320
  69.8 0.6 copy.9
